TPU v7x, 256 devices: a whole 4x4x8 slice. The times are simulated.
256 devices in a mesh: sp: 64 (over z, y, core), tp: 4 (over x).
Axes of the slice: x: 4, y: 4, z: 8, core: 2. Of those that a mesh axis runs over, the one named last changes fastest.
Arguments:
- out_grad: bfloat16 [12288, 2048], P('sp'), may hold values from -16 to 16
- routes: int32 [12288, 2], P('sp'), may hold values from 0 to 63, all different within a row; in each aligned block of 192 rows (0 to 191, 192 to 383, ...) at most 12 rows name the same one
- route_weight: float32 [12288, 2], P('sp'), may hold values from 0.3 to 1.5
- expert_rows: bfloat16 [64, 64, 12, 2048], P(None, 'sp'), may hold values from -6 to 6
- gate_weight: bfloat16 [64, 2048, 1024], P('sp', None, 'tp'), may hold values from -0.125 to 0.125
- up_weight: bfloat16 [64, 2048, 1024], P('sp', None, 'tp'), may hold values from -0.125 to 0.125
- down_weight: bfloat16 [64, 1024, 2048], P('sp', 'tp'), may hold values from -0.1875 to 0.1875
- conv_input: bfloat16 [12288, 1024], P('sp', 'tp'), may hold values from -6 to 6
- out_gate: bfloat16 [12288, 1024], P('sp', 'tp'), may hold values from -6 to 6
- in_gate: bfloat16 [12288, 1024], P('sp', 'tp'), may hold values from -6 to 6
- taps: float32 [3, 1024], P(None, 'tp'), may hold values from -3 to 3
- out_weight: bfloat16 [2048, 1024], P(None, 'tp'), may hold values from -0.1875 to 0.1875
Outputs:
- gate_grad: bfloat16 [64, 2048, 1024], P('sp', None, 'tp')
- up_grad: bfloat16 [64, 2048, 1024], P('sp', None, 'tp')
- down_grad: bfloat16 [64, 1024, 2048], P('sp', 'tp')
- mid_grad: bfloat16 [12288, 2048], P('sp', 'tp')
- out_weight_grad: float32 [2048, 1024], P('sp', 'tp')
- input_grad: bfloat16 [12288, 1024], P('sp', 'tp')
- out_gate_grad: bfloat16 [12288, 1024], P('sp', 'tp')
- in_gate_grad: bfloat16 [12288, 1024], P('sp', 'tp')
Inputs may be any that keep to these rules, and one draw needn't show every extreme that they name: `routes`: each token names 2 different experts; within each aligned block of 192 tokens no expert is named by more than 12 tokens, a bound that some block reaches.
All inputs are finite; a program needn't handle non-finite values.
Results may differ from a plain program's by a relative error of at most 0.014.
Values may be sent and summed in bfloat16 or wider, within the bound.
No kernel may reach another device: no remote copies, remote signals or barrier semaphores. Data moves between devices by JAX's collectives and lax.ppermute only.
A program may use at most 64 MiB of HBM per device.

v0:
```python
import jax
import jax.numpy as jnp
from jax import lax
from jax.sharding import PartitionSpec as P


def split_up(shard, dim, peers):
    shape = shard.shape
    pieces = shard.reshape(*shape[:dim], peers, shape[dim] // peers, *shape[dim + 1 :])
    return jnp.moveaxis(pieces, dim, 0)


def sum_at_owner(shard, axis, dim):
    peers = lax.axis_size(axis)
    pieces = lax.all_to_all(split_up(shard, dim, peers), axis, 0, 0, tiled=True)
    return jnp.sum(pieces.astype(jnp.float32), axis=0)


def passed_along(shard, axis, by):
    peers = lax.axis_size(axis)
    pairs = [(i, i + by) for i in range(peers) if 0 <= i + by < peers]
    return lax.ppermute(shard, axis, pairs)


def on_device(
    out_grad,
    routes,
    route_weight,
    expert_rows,
    gate_weight,
    up_weight,
    down_weight,
    conv_input,
    out_gate,
    in_gate,
    taps,
    out_weight,
):
    groups = lax.axis_size("tp")
    member = lax.axis_index("tp")
    sources = lax.axis_size("sp")
    tok_rows, width = out_grad.shape
    top = routes.shape[1]
    local = gate_weight.shape[0]
    experts = local * sources
    slots = expert_rows.shape[2]
    share = width // groups
    flat = routes.reshape(-1)
    onehot = (flat[:, None] == jnp.arange(experts, dtype=jnp.int32)[None, :]).astype(jnp.int32)
    place = jnp.sum((jnp.cumsum(onehot, axis=0) - onehot) * onehot, axis=1)
    target = flat * slots + place
    slot_grad = (route_weight[:, :, None] * out_grad[:, None, :].astype(jnp.float32)).astype(
        jnp.bfloat16
    )
    outgoing = (
        jnp.zeros((experts * slots, width), jnp.bfloat16)
        .at[target]
        .set(slot_grad.reshape(-1, width))
    )
    outgoing = outgoing.reshape(sources, local, slots, width)
    portion = slots // groups
    piece = lax.dynamic_slice_in_dim(outgoing, member * portion, portion, 2)
    arrived = lax.all_to_all(piece, "sp", split_axis=0, concat_axis=0, tiled=True)
    grads = lax.all_gather(arrived, "tp", axis=2, tiled=True)
    gate = jnp.einsum(
        "secd,edf->secf", expert_rows, gate_weight, preferred_element_type=jnp.float32
    )
    up = jnp.einsum("secd,edf->secf", expert_rows, up_weight, preferred_element_type=jnp.float32)
    sig = jax.nn.sigmoid(gate)
    act = (gate * sig * up).astype(jnp.bfloat16)
    act_grad = jnp.einsum("secd,efd->secf", grads, down_weight, preferred_element_type=jnp.float32)
    up_part = (act_grad * gate * sig).astype(jnp.bfloat16)
    gate_part = (act_grad * up * sig * (1.0 + gate * (1.0 - sig))).astype(jnp.bfloat16)
    down_grad = jnp.einsum("secf,secd->efd", act, grads, preferred_element_type=jnp.float32).astype(
        jnp.bfloat16
    )
    gate_grad = jnp.einsum(
        "secd,secf->edf", expert_rows, gate_part, preferred_element_type=jnp.float32
    ).astype(jnp.bfloat16)
    up_grad = jnp.einsum(
        "secd,secf->edf", expert_rows, up_part, preferred_element_type=jnp.float32
    ).astype(jnp.bfloat16)
    row_part = jnp.einsum(
        "secf,edf->secd", gate_part, gate_weight, preferred_element_type=jnp.float32
    )
    row_part = row_part + jnp.einsum(
        "secf,edf->secd", up_part, up_weight, preferred_element_type=jnp.float32
    )
    summed = sum_at_owner(row_part.astype(jnp.bfloat16), "tp", 3)
    returned = lax.all_to_all(
        summed.astype(jnp.bfloat16), "sp", split_axis=0, concat_axis=0, tiled=True
    )
    returned = returned.reshape(experts * slots, share)
    picked = (
        jnp.take(returned, target, axis=0)
        .astype(jnp.float32)
        .reshape(tok_rows, top, share)
        .sum(axis=1)
    )
    own_cols = lax.dynamic_slice_in_dim(out_grad, member * share, share, 1).astype(jnp.float32)
    mid_grad = (own_cols + picked).astype(jnp.bfloat16)
    mid_whole = lax.all_gather(mid_grad, "tp", axis=1, tiled=True)
    reach = taps.shape[0] - 1
    rims = jnp.stack([in_gate[tok_rows - reach :], conv_input[tok_rows - reach :]])
    prior = passed_along(rims, "sp", 1)
    mixed = in_gate.astype(jnp.float32) * conv_input.astype(jnp.float32)
    prior_mixed = prior[0].astype(jnp.float32) * prior[1].astype(jnp.float32)
    extended = jnp.concatenate([prior_mixed, mixed], axis=0)
    conv = jnp.zeros_like(mixed)
    for tap in range(reach + 1):
        conv = conv + taps[tap][None, :] * extended[reach - tap : reach - tap + tok_rows]
    gated = (out_gate.astype(jnp.float32) * conv).astype(jnp.bfloat16)
    out_weight_grad = sum_at_owner(
        lax.dot_general(
            mid_whole, gated, (((0,), (0,)), ((), ())), preferred_element_type=jnp.float32
        ).astype(jnp.bfloat16),
        "sp",
        0,
    )
    gated_grad = jnp.dot(mid_whole, out_weight, preferred_element_type=jnp.float32)
    out_gate_grad = (gated_grad * conv).astype(jnp.bfloat16)
    conv_grad = gated_grad * out_gate.astype(jnp.float32)
    later = passed_along(conv_grad[:reach], "sp", -1)
    following = jnp.concatenate([conv_grad, later], axis=0)
    mixed_grad = jnp.zeros_like(conv_grad)
    for tap in range(reach + 1):
        mixed_grad = mixed_grad + taps[tap][None, :] * following[tap : tap + tok_rows]
    input_grad = (mixed_grad * in_gate.astype(jnp.float32)).astype(jnp.bfloat16)
    in_gate_grad = (mixed_grad * conv_input.astype(jnp.float32)).astype(jnp.bfloat16)
    return (
        gate_grad,
        up_grad,
        down_grad,
        mid_grad,
        out_weight_grad,
        input_grad,
        out_gate_grad,
        in_gate_grad,
    )


def solution(mesh):
    in_specs = (
        P("sp", None),
        P("sp", None),
        P("sp", None),
        P(None, "sp", None, None),
        P("sp", None, "tp"),
        P("sp", None, "tp"),
        P("sp", "tp", None),
        P("sp", "tp"),
        P("sp", "tp"),
        P("sp", "tp"),
        P(None, "tp"),
        P(None, "tp"),
    )
    out_specs = (
        P("sp", None, "tp"),
        P("sp", None, "tp"),
        P("sp", "tp", None),
        P("sp", "tp"),
        P("sp", "tp"),
        P("sp", "tp"),
        P("sp", "tp"),
        P("sp", "tp"),
    )
    return jax.shard_map(
        on_device, mesh=mesh, in_specs=in_specs, out_specs=out_specs, check_vma=False
    )
```

profile of v0, /device:TPU:1, one launch (start us, length us, event | category | flops | bytes accessed | tf_op | source)
XLA Modules:
  0.0 281.8 jit_solution(15357142444350941405)
XLA Ops:
  10.7 4.4 %mul.148 = f32[192,2,2048]{2,1,0:T(2,128)} broadcast(bf16[192,2048]{1,0:T(8,128)(2,1)} %param.12), dimensions={0,2} | broadcast | bytes 3932160 | tf_op jit(solution)/shard_map/mul | solution.py:52
  15.1 5.3 %mul.149 = f32[384,2048]{1,0:T(8,128)} reshape(f32[192,2,2048]{2,1,0:T(2,128)} %mul.148) | data formatting | bytes 6291456 | tf_op jit(solution)/shard_map/mul | solution.py:52
  20.8 6.4 %scatter_custom_fusion = bf16[768,2048]{1,0:T(8,128)(2,1)} fusion(s32[384]{0:T(512)S(1)} %fusion.80, f32[384,2048]{1,0:T(8,128)} %mul.149, f32[384]{0:T(512)S(1)} %mul.146, bf16[]{:T(256)} %constant.12.clone.1), kind=kCustom, calls=%fused_computation.28 | custom fusion | flops 1572864 | bytes 6293506 | tf_op jit(solution)/shard_map/scatter | solution.py:58
  27.2 6.1 %reshape.145 = bf16[64,1,12,2048]{3,2,0,1:T(8,128)(2,1)} reshape(bf16[768,2048]{1,0:T(8,128)(2,1)} %scatter_custom_fusion) | data formatting | bytes 6291456 | tf_op jit(solution)/shard_map/reshape | solution.py:60
  33.2 3.0 %dynamic-slice_bitcast_fusion = bf16[64,1,3,2048]{3,2,1,0:T(4,128)(2,1)S(1)} fusion(bf16[64,1,12,2048]{3,2,0,1:T(8,128)(2,1)} %reshape.145, s32[]{:T(128)S(6)} %select_n.30), kind=kLoop, calls=%fused_computation.40 | loop fusion | bytes 1572868 | tf_op jit(solution)/shard_map/dynamic_slice | solution.py:62
  36.3 41.1 %all_to_all.20 = bf16[64,1,3,2048]{3,2,1,0:T(4,128)(2,1)S(1)} all-to-all(bf16[64,1,3,2048]{3,2,1,0:T(4,128)(2,1)S(1)} %dynamic-slice_bitcast_fusion), channel_id=1, replica_groups=mesh['sp'=64,'tp'=4] {'sp'}, dimensions={0} | all-to-all | bytes 1572864 | tf_op jit(solution)/shard_map/all_to_all | solution.py:63
  77.4 1.5 copy.49
  78.9 3.2 %fusion.48 = f32[64,1,12,256]{3,0,2,1:T(8,128)} fusion(bf16[64,1,12,2048]{3,0,2,1:T(8,128)(2,1)S(1)} %copy-done, bf16[1,2048,256]{2,1,0:T(8,128)(2,1)} %param.16), kind=kOutput, calls=%fused_computation.33 | convolution fusion | flops 805306368 | bytes 4980736 | tf_op jit(solution)/shard_map/secd,edf->secf/dot_general | solution.py:65
  82.1 1.9 fusion.45
  84.0 33.8 %all-gather.2.cloned.1.call-done = bf16[64,1,12,2048]{3,0,1,2:T(8,128)(2,1)} async-done(((bf16[64,1,3,2048]{3,0,1,2:T(8,128)(2,1)}), bf16[64,1,12,2048]{3,0,1,2:T(8,128)(2,1)}) %all-gather.2.cloned.1.call-update) | async-done | bytes 3145744 | tf_op jit(solution)/shard_map/all_gather | solution.py:64
  117.8 3.9 %multiply_convert_fusion.3 = (bf16[64,1,12,256]{3,0,2,1:T(8,128)(2,1)S(1)}, bf16[64,1,12,256]{3,0,2,1:T(8,128)(2,1)S(1)}) fusion(f32[64,1,12,256]{3,0,2,1:T(8,128)} %fusion.48, f32[64,1,12,256]{3,0,2,1:T(8,128)} %fusion.45, bf16[1,256,2048]{2,1,0:T(8,128)(2,1)} %param.18, bf16[64,1,12,2048]{3,0,1,2:T(8,128)(2,1)} %all-gather.2.cloned.1.call-done), kind=kOutput, calls=%fused_computation.43 | convolution fusion | flops 807862272 | bytes 6553600 | tf_op jit(solution)/shard_map/secd,efd->secf/dot_general | solution.py:71
  124.6 39.9 %all_to_all.21 = bf16[4,64,1,12,512]{4,1,3,2,0:T(8,128)(2,1)} all-to-all(bf16[4,64,1,12,512]{4,1,3,2,0:T(8,128)(2,1)S(1)} %bitcast.161), channel_id=1, replica_groups=mesh['sp'=64,'tp'=4] {'tp'}, dimensions={0} | all-to-all | bytes 6291456 | tf_op jit(solution)/shard_map/all_to_all | solution.py:15
  164.5 3.5 %reduce_sum.48 = bf16[64,12,512]{2,0,1:T(8,128)(2,1)} reduce(bf16[4,64,1,12,512]{4,1,3,2,0:T(8,128)(2,1)} %all_to_all.21, bf16[]{:T(256)} %constant.12.clone.1), dimensions={0,2}, to_apply=%region_4.5 | reduce | flops 1179648 | bytes 3932162 | tf_op jit(solution)/shard_map/reduce_sum | solution.py:16
  168.1 2.5 copy.54
  170.6 12.1 %all-to-all-start.2 = ((bf16[64,1,12,512]{3,2,1,0:T(8,128)(2,1)}), bf16[64,1,12,512]{3,2,1,0:T(8,128)(2,1)}, u32[]{:S(2)}, u32[]{:S(2)}) async-start(bf16[64,1,12,512]{3,2,1,0:T(8,128)(2,1)} %copy.54), calls=%async_computation.2 | async-start | bytes 2097152 | tf_op jit(solution)/shard_map/all_to_all | solution.py:90
  182.8 3.5 %collective-permute-start = (bf16[2,2,256]{2,1,0:T(2,128)(2,1)S(1)}, bf16[2,2,256]{2,1,0:T(2,128)(2,1)S(1)}, u32[]{:S(2)}, u32[]{:S(2)}) collective-permute-start(bf16[2,2,256]{2,1,0:T(2,128)(2,1)S(1)} %pad_maximum_fusion.2), channel_id=1, source_target_pairs={{0,4},{4,8},{8,12},{12,16},{16,20},{20,24},{24,28},{28,32},{32,36}... | collective-permute-start | bytes 6152 | tf_op jit(solution)/shard_map/ppermute | solution.py:22
  188.6 22.2 %all-to-all-done.2 = bf16[64,1,12,512]{3,2,1,0:T(8,128)(2,1)} async-done(((bf16[64,1,12,512]{3,2,1,0:T(8,128)(2,1)}), bf16[64,1,12,512]{3,2,1,0:T(8,128)(2,1)}, u32[]{:S(2)}, u32[]{:S(2)}) %all-to-all-start.2) | async-done | bytes 786464 | tf_op jit(solution)/shard_map/all_to_all | solution.py:90
  210.8 2.1 reshape.155
  212.9 3.3 %gather_fusion = bf16[384,512]{1,0:T(8,128)(2,1)S(1)} fusion(bf16[768,512]{1,0:T(8,128)(2,1)} %reshape.155, s32[1024]{0:T(1024)S(1)} %pad_clamp_fusion), kind=kCustom, calls=%fused_computation | custom fusion | bytes 787968 | tf_op jit(solution)/shard_map/jit(_take)/gather | solution.py:95
  217.1 2.2 convert_reduce_fusion.1
  220.3 11.0 %all_gather.7 = bf16[192,2048]{1,0:T(8,128)(2,1)S(1)} all-gather(bf16[192,512]{1,0:T(8,128)(2,1)S(1)} %add_convert_fusion.1), channel_id=1, replica_groups=mesh['sp'=64,'tp'=4] {'tp'}, dimensions={1}, use_global_device_ids=true | all-gather | bytes 983040 | tf_op jit(solution)/shard_map/all_gather | solution.py:102
  231.3 2.5 multiply_convert_fusion.6
  233.7 1.5 convolution_convert_fusion
  235.2 9.6 %all-to-all-start.3 = ((bf16[64,32,256]{2,1,0:T(8,128)(2,1)}), bf16[64,32,256]{2,1,0:T(8,128)(2,1)}, u32[]{:S(2)}, u32[]{:S(2)}) async-start(bf16[64,32,256]{2,1,0:T(8,128)(2,1)} %bitcast.163), calls=%async_computation.3 | async-start | bytes 2097152 | tf_op jit(solution)/shard_map/all_to_all | solution.py:15
  244.9 3.1 %fusion.33 = bf16[1,2048,256]{1,2,0:T(8,128)(2,1)} fusion(bf16[64,1,12,2048]{3,0,2,1:T(8,128)(2,1)S(1)} %copy-done, bf16[64,1,12,256]{3,0,2,1:T(8,128)(2,1)} %copy-done.12), kind=kOutput, calls=%fused_computation.25 | convolution fusion | flops 805830656 | bytes 4587520 | tf_op jit(solution)/shard_map/secd,secf->edf/dot_general | solution.py:77
  248.0 2.0 fusion.30
  250.6 2.4 collective-permute-start.1
  253.1 2.0 fusion.36
  255.1 2.3 copy.55
  257.4 2.3 copy.56
  261.0 11.9 %all-to-all-done.3 = bf16[64,32,256]{2,1,0:T(8,128)(2,1)} async-done(((bf16[64,32,256]{2,1,0:T(8,128)(2,1)}), bf16[64,32,256]{2,1,0:T(8,128)(2,1)}, u32[]{:S(2)}, u32[]{:S(2)}) %all-to-all-start.3) | async-done | bytes 1048608 | tf_op jit(solution)/shard_map/all_to_all | solution.py:15
  272.9 2.0 convert_reduce_fusion
  (76 shorter events, 12.9 us)
Async XLA Ops:
  7.2 71.7 %copy-start = (bf16[64,1,12,2048]{3,0,2,1:T(8,128)(2,1)S(1)}, bf16[64,1,12,2048]{3,0,2,1:T(8,128)(2,1)}, u32[]{:S(2)}) copy-start(bf16[64,1,12,2048]{3,0,2,1:T(8,128)(2,1)} %param.15) | copy-start | bytes 9437188
  7.2 110.6 %all-gather.2.cloned.1.call-start = ((), (), s32[]{:S(2)}) async-start(), calls=%async_computation.4 | async-start | bytes 3932160 | tf_op jit(solution)/shard_map/all_gather | solution.py:64
  15.1 5.3 %copy-start.16 = (f32[192,2]{0,1:T(2,128)S(1)}, f32[192,2]{0,1:T(2,128)}, u32[]{:S(2)}) copy-start(f32[192,2]{0,1:T(2,128)} %param.14) | copy-start | bytes 4612
  78.9 3.2 %copy-start.2 = (bf16[1,2048,256]{2,1,0:T(8,128)(2,1)S(1)}, bf16[1,2048,256]{2,1,0:T(8,128)(2,1)}, u32[]{:S(2)}) copy-start(bf16[1,2048,256]{2,1,0:T(8,128)(2,1)} %param.17) | copy-start | bytes 3145732
  117.8 3.9 %copy-start.1 = (bf16[1,2048,256]{2,1,0:T(8,128)(2,1)S(1)}, bf16[1,2048,256]{2,1,0:T(8,128)(2,1)}, u32[]{:S(2)}) copy-start(bf16[1,2048,256]{2,1,0:T(8,128)(2,1)} %param.16) | copy-start | bytes 3145732
  121.7 1.1 copy-start.12
  121.7 1.1 copy-start.10
  121.7 1.5 copy-start.3
  164.5 18.2 %copy-start.5 = (bf16[192,256]{1,0:T(8,128)(2,1)S(1)}, bf16[192,256]{1,0:T(8,128)(2,1)}, u32[]{:S(2)}) copy-start(bf16[192,256]{1,0:T(8,128)(2,1)} %param.19) | copy-start | bytes 294916
  164.5 18.2 %copy-start.7 = (bf16[192,256]{1,0:T(8,128)(2,1)S(1)}, bf16[192,256]{1,0:T(8,128)(2,1)}, u32[]{:S(2)}) copy-start(bf16[192,256]{1,0:T(8,128)(2,1)} %param.21) | copy-start | bytes 294916
  164.5 22.0 %copy-start.13 = (s32[192,2]{0,1:T(2,128)S(1)}, s32[192,2]{0,1:T(2,128)}, u32[]{:S(2)}) copy-start(s32[192,2]{0,1:T(2,128)} %param.13) | copy-start | bytes 4612
  164.5 22.1 %copy-start.15 = (f32[3,256]{1,0:T(4,128)S(1)}, f32[3,256]{1,0:T(4,128)}, u32[]{:S(2)}) copy-start(f32[3,256]{1,0:T(4,128)} %param.22) | copy-start | bytes 9220
  170.6 40.2 %all-to-all-start.2 = ((bf16[64,1,12,512]{3,2,1,0:T(8,128)(2,1)}), bf16[64,1,12,512]{3,2,1,0:T(8,128)(2,1)}, u32[]{:S(2)}, u32[]{:S(2)}) async-start(bf16[64,1,12,512]{3,2,1,0:T(8,128)(2,1)} %copy.54), calls=%async_computation.2 | async-start | bytes 2097152 | tf_op jit(solution)/shard_map/all_to_all | solution.py:90
  182.8 5.3 %collective-permute-start = (bf16[2,2,256]{2,1,0:T(2,128)(2,1)S(1)}, bf16[2,2,256]{2,1,0:T(2,128)(2,1)S(1)}, u32[]{:S(2)}, u32[]{:S(2)}) collective-permute-start(bf16[2,2,256]{2,1,0:T(2,128)(2,1)S(1)} %pad_maximum_fusion.2), channel_id=1, source_target_pairs={{0,4},{4,8},{8,12},{12,16},{16,20},{20,24},{24,28},{28,32},{32,36}... | collective-permute-start | bytes 6152 | tf_op jit(solution)/shard_map/ppermute | solution.py:22
  216.2 15.1 %copy-start.14 = (f32[2,256]{1,0:T(2,128)S(1)}, f32[2,256]{1,0:T(2,128)}, u32[]{:S(2)}) copy-start(f32[2,256]{1,0:T(2,128)} %multiply_bitcast_fusion) | copy-start | bytes 6148
  217.1 16.6 %copy-start.9 = (bf16[192,256]{1,0:T(8,128)(2,1)S(1)}, bf16[192,256]{1,0:T(8,128)(2,1)}, u32[]{:S(2)}) copy-start(bf16[192,256]{1,0:T(8,128)(2,1)} %param.20) | copy-start | bytes 294916
  220.3 14.9 %copy-start.4 = (bf16[192,512]{1,0:T(8,128)(2,1)}, bf16[192,512]{1,0:T(8,128)(2,1)S(1)}, u32[]{:S(2)}) copy-start(bf16[192,512]{1,0:T(8,128)(2,1)S(1)} %add_convert_fusion.1) | copy-start | bytes 589828
  235.2 37.7 %all-to-all-start.3 = ((bf16[64,32,256]{2,1,0:T(8,128)(2,1)}), bf16[64,32,256]{2,1,0:T(8,128)(2,1)}, u32[]{:S(2)}, u32[]{:S(2)}) async-start(bf16[64,32,256]{2,1,0:T(8,128)(2,1)} %bitcast.163), calls=%async_computation.3 | async-start | bytes 2097152 | tf_op jit(solution)/shard_map/all_to_all | solution.py:15
  244.9 3.2 %copy-start.17 = (bf16[64,1,12,2048]{3,0,1,2:T(8,128)(2,1)S(1)}, bf16[64,1,12,2048]{3,0,1,2:T(8,128)(2,1)}, u32[]{:S(2)}) copy-start(bf16[64,1,12,2048]{3,0,1,2:T(8,128)(2,1)} %all-gather.2.cloned.1.call-done) | copy-start | bytes 9437188
  244.9 3.1 %copy-start.18 = (f32[64,1,12,256]{3,0,2,1:T(8,128)S(1)}, f32[64,1,12,256]{3,0,2,1:T(8,128)}, u32[]{:S(2)}) copy-start(f32[64,1,12,256]{3,0,2,1:T(8,128)} %fusion.48) | copy-start | bytes 2359300
  244.9 3.1 %copy-start.19 = (f32[64,1,12,256]{3,0,2,1:T(8,128)S(1)}, f32[64,1,12,256]{3,0,2,1:T(8,128)}, u32[]{:S(2)}) copy-start(f32[64,1,12,256]{3,0,2,1:T(8,128)} %fusion.45) | copy-start | bytes 2359300
  248.0 5.1 %copy-start.11 = (bf16[64,1,12,256]{3,0,2,1:T(8,128)(2,1)S(1)}, bf16[64,1,12,256]{3,0,2,1:T(8,128)(2,1)}, u32[]{:S(2)}) copy-start(bf16[64,1,12,256]{3,0,2,1:T(8,128)(2,1)} %copy-done.10) | copy-start | bytes 1179652
  250.6 9.0 %collective-permute-start.1 = (f32[2,256]{1,0:T(2,128)}, f32[2,256]{1,0:T(2,128)S(1)}, u32[]{:S(2)}, u32[]{:S(2)}) collective-permute-start(f32[2,256]{1,0:T(2,128)} %slice.66), channel_id=1, source_target_pairs={{4,0},{8,4},{12,8},{16,12},{20,16},{24,20},{28,24},{32,28},{36,32}... | collective-permute-start | bytes 6152 | tf_op jit(solution)/shard_map/ppermute | solution.py:22
  255.1 4.6 %copy-start.6 = (bf16[192,256]{1,0:T(8,128)(2,1)S(1)}, bf16[192,256]{1,0:T(8,128)(2,1)}, u32[]{:S(2)}) copy-start(bf16[192,256]{1,0:T(8,128)(2,1)} %param.19) | copy-start | bytes 294916
  255.1 5.3 %copy-start.8 = (bf16[192,256]{1,0:T(8,128)(2,1)S(1)}, bf16[192,256]{1,0:T(8,128)(2,1)}, u32[]{:S(2)}) copy-start(bf16[192,256]{1,0:T(8,128)(2,1)} %param.21) | copy-start | bytes 294916
Sparse Core Ops, SparseCore 0:
  79.0 38.7 all-gather.1
where the time goes:
time: 283 us; the launch traced here: 282 us
  blocking collectives  92 us (33%)
  waiting for transfers between devices  67.9 us (24%)
  local copies, waits for them, and re-layouts  37.9 us (13%)
  starting transfers between devices  27.8 us (10%)
  matrix products  22 us (8%)
  other arithmetic  19.7 us (7%)
  between operations  14.4 us (5%)
    all_to_all x1, blocking collectives, on_device(): lax.all_to_all(piece, 'sp', split_axis=0, concat_axis=0, tiled=True)  41.1 us
    all_to_all x1, blocking collectives, sum_at_owner(): pieces = lax.all_to_all(split_up(shard, dim, peers), axis, 0, 0, tiled=True)  39.9 us
    all_gather x1, waiting for transfers between devices, on_device(): grads = lax.all_gather(arrived, 'tp', axis=2, tiled=True)  33.8 us
    all_to_all x1, waiting for transfers between devices, on_device(): lax.all_to_all(summed.astype(jnp.bfloat16), 'sp', split_axis=0, concat_ax...  22.2 us
    all_to_all x1, starting transfers between devices, on_device(): lax.all_to_all(summed.astype(jnp.bfloat16), 'sp', split_axis=0, concat_ax...  12.1 us
    all_to_all x1, waiting for transfers between devices, sum_at_owner(): pieces = lax.all_to_all(split_up(shard, dim, peers), axis, 0, 0, tiled=True)  11.9 us
    all_gather x1, blocking collectives, on_device(): mid_whole = lax.all_gather(mid_grad, 'tp', axis=1, tiled=True)  11 us
    mul x3, local copies, waits for them, and re-layouts, on_device(): route_weight[:, :, None] * out_grad[:, None, :].astype(jnp.float32)  9.84 us
  transfers between devices with their start and end apart: 5, of which 3 were waited for; matrix products, arithmetic and copies ran while one was open for 7% of the time, Pallas kernels for 0%

commit v1 on v0

--- a/solution.py
+++ b/solution.py
@@ -2,6 +2,14 @@
 import jax.numpy as jnp
 from jax import lax
 from jax.sharding import PartitionSpec as P
+
+
+def gather_by_exchange(array, axis, dim):
+    peers = lax.axis_size(axis)
+    repeats = [peers if d == dim else 1 for d in range(array.ndim)]
+    return lax.all_to_all(
+        jnp.tile(array, repeats), axis, split_axis=dim, concat_axis=dim, tiled=True
+    )
 
 
 def split_up(shard, dim, peers):
@@ -61,7 +69,7 @@
     portion = slots // groups
     piece = lax.dynamic_slice_in_dim(outgoing, member * portion, portion, 2)
     arrived = lax.all_to_all(piece, "sp", split_axis=0, concat_axis=0, tiled=True)
-    grads = lax.all_gather(arrived, "tp", axis=2, tiled=True)
+    grads = gather_by_exchange(arrived, "tp", 2)
     gate = jnp.einsum(
         "secd,edf->secf", expert_rows, gate_weight, preferred_element_type=jnp.float32
     )

time: 283 us -> 269 us (0.951)
  between operations: 14.4 us -> 0.98 us
  waiting for transfers between devices: 67.9 us -> 63.5 us
    all_gather x1 -> x0, waiting for transfers between devices: 33.8 us -> none  [on_device(): grads = lax.all_gather(arrived, 'tp', axis=2, tiled=True)]
    all_to_all x0 -> x1, waiting for transfers between devices: none -> 31.3 us  [gather_by_exchange(): lax.all_to_all(jnp.tile(array, repeats), axis, split_axis=dim, concat_axi...]
    all_to_all x0 -> x1, starting transfers between devices: none -> 4.83 us  [gather_by_exchange(): lax.all_to_all(jnp.tile(array, repeats), axis, split_axis=dim, concat_axi...]
    unnamed x44 -> x42, local copies, waits for them, and re-layouts: 6.07 us -> 6.11 us
  transfers between devices with their start and end apart: 5 -> 5, of which waited for: 3 -> 3; matrix products, arithmetic and copies ran while one was open for 7% -> 9% of each run, Pallas kernels for 0% -> 0%
where the time goes in v1:
time: 269 us; the launch traced here: 268 us
  blocking collectives  90.8 us (34%)
  waiting for transfers between devices  63.5 us (24%)
  local copies, waits for them, and re-layouts  39.2 us (15%)
  starting transfers between devices  29.9 us (11%)
  matrix products  24 us (9%)
  other arithmetic  19.8 us (7%)
    all_to_all x1, blocking collectives, on_device(): lax.all_to_all(piece, 'sp', split_axis=0, concat_axis=0, tiled=True)  41.1 us
    all_to_all x1, blocking collectives, sum_at_owner(): pieces = lax.all_to_all(split_up(shard, dim, peers), axis, 0, 0, tiled=True)  38.7 us
    all_to_all x1, waiting for transfers between devices, gather_by_exchange(): lax.all_to_all(jnp.tile(array, repeats), axis, split_axis=dim, concat_axi...  31.3 us
    all_to_all x1, waiting for transfers between devices, on_device(): lax.all_to_all(summed.astype(jnp.bfloat16), 'sp', split_axis=0, concat_ax...  22.2 us
    all_gather x1, blocking collectives, on_device(): mid_whole = lax.all_gather(mid_grad, 'tp', axis=1, tiled=True)  11 us
    all_to_all x1, waiting for transfers between devices, sum_at_owner(): pieces = lax.all_to_all(split_up(shard, dim, peers), axis, 0, 0, tiled=True)  10 us
    mul x3, local copies, waits for them, and re-layouts, on_device(): route_weight[:, :, None] * out_grad[:, None, :].astype(jnp.float32)  9.85 us
    all_to_all x1, starting transfers between devices, sum_at_owner(): pieces = lax.all_to_all(split_up(shard, dim, peers), axis, 0, 0, tiled=True)  9.48 us
  transfers between devices with their start and end apart: 5, of which 3 were waited for; matrix products, arithmetic and copies ran while one was open for 9% of the time, Pallas kernels for 0%

profile of v1, /device:TPU:1, one launch (start us, length us, event | category | flops | bytes accessed | tf_op | source)
XLA Modules:
  0.0 268.0 jit_solution(3812791939933531819)
XLA Ops:
  4.2 4.4 %mul.148 = f32[192,2,2048]{2,1,0:T(2,128)} broadcast(bf16[192,2048]{1,0:T(8,128)(2,1)} %param.12), dimensions={0,2} | broadcast | bytes 3932160 | tf_op jit(solution)/shard_map/mul | solution.py:60
  8.6 5.3 %mul.149 = f32[384,2048]{1,0:T(8,128)} reshape(f32[192,2,2048]{2,1,0:T(2,128)} %mul.148) | data formatting | bytes 6291456 | tf_op jit(solution)/shard_map/mul | solution.py:60
  14.3 6.4 %scatter_custom_fusion = bf16[768,2048]{1,0:T(8,128)(2,1)} fusion(s32[384]{0:T(512)S(1)} %fusion.80, f32[384,2048]{1,0:T(8,128)} %mul.149, f32[384]{0:T(512)S(1)} %mul.146, bf16[]{:T(256)} %constant.12.clone.1), kind=kCustom, calls=%fused_computation.28 | custom fusion | flops 1572864 | bytes 6293506 | tf_op jit(solution)/shard_map/scatter | solution.py:66
  20.7 6.1 %reshape.151 = bf16[64,1,12,2048]{3,2,0,1:T(8,128)(2,1)} reshape(bf16[768,2048]{1,0:T(8,128)(2,1)} %scatter_custom_fusion) | data formatting | bytes 6291456 | tf_op jit(solution)/shard_map/reshape | solution.py:68
  26.7 3.0 %dynamic-slice_bitcast_fusion = bf16[64,1,3,2048]{3,2,1,0:T(4,128)(2,1)S(1)} fusion(bf16[64,1,12,2048]{3,2,0,1:T(8,128)(2,1)} %reshape.151, s32[]{:T(128)S(6)} %select_n.30), kind=kLoop, calls=%fused_computation.40 | loop fusion | bytes 1572868 | tf_op jit(solution)/shard_map/dynamic_slice | solution.py:70
  29.8 41.1 %all_to_all.25 = bf16[64,1,3,2048]{3,2,1,0:T(4,128)(2,1)S(1)} all-to-all(bf16[64,1,3,2048]{3,2,1,0:T(4,128)(2,1)S(1)} %dynamic-slice_bitcast_fusion), channel_id=1, replica_groups=mesh['sp'=64,'tp'=4] {'sp'}, dimensions={0} | all-to-all | bytes 1572864 | tf_op jit(solution)/shard_map/all_to_all | solution.py:71
  71.4 2.1 tile.12
  73.5 4.8 %all-to-all-start.1 = ((bf16[64,1,12,2048]{3,0,1,2:T(8,128)(2,1)}), bf16[64,1,12,2048]{3,0,1,2:T(8,128)(2,1)}, u32[]{:S(2)}, u32[]{:S(2)}) async-start(bf16[64,1,12,2048]{3,0,1,2:T(8,128)(2,1)} %bitcast.164), calls=%async_computation.1 | async-start | bytes 6291456 | tf_op jit(solution)/shard_map/all_to_all | solution.py:10
  78.4 3.2 %fusion.48 = f32[64,1,12,256]{3,0,2,1:T(8,128)} fusion(bf16[64,1,12,2048]{3,0,2,1:T(8,128)(2,1)S(1)} %copy-done, bf16[1,2048,256]{2,1,0:T(8,128)(2,1)} %param.16), kind=kOutput, calls=%fused_computation.33 | convolution fusion | flops 805306368 | bytes 4980736 | tf_op jit(solution)/shard_map/secd,edf->secf/dot_general | solution.py:73
  81.6 1.9 fusion.45
  83.4 31.3 %all-to-all-done.1 = bf16[64,1,12,2048]{3,0,1,2:T(8,128)(2,1)} async-done(((bf16[64,1,12,2048]{3,0,1,2:T(8,128)(2,1)}), bf16[64,1,12,2048]{3,0,1,2:T(8,128)(2,1)}, u32[]{:S(2)}, u32[]{:S(2)}) %all-to-all-start.1) | async-done | bytes 3145760 | tf_op jit(solution)/shard_map/all_to_all | solution.py:10
  114.7 3.9 %multiply_convert_fusion.3 = (bf16[64,1,12,256]{3,0,2,1:T(8,128)(2,1)S(1)}, bf16[64,1,12,256]{3,0,2,1:T(8,128)(2,1)S(1)}) fusion(f32[64,1,12,256]{3,0,2,1:T(8,128)} %fusion.48, f32[64,1,12,256]{3,0,2,1:T(8,128)} %fusion.45, bf16[1,256,2048]{2,1,0:T(8,128)(2,1)} %param.18, bf16[64,1,12,2048]{3,0,1,2:T(8,128)(2,1)} %all-to-all-done.1), kind=kOutput, calls=%fused_computation.43 | convolution fusion | flops 807862272 | bytes 6553600 | tf_op jit(solution)/shard_map/secd,efd->secf/dot_general | solution.py:79
  121.6 38.7 %all_to_all.26 = bf16[4,64,1,12,512]{4,1,3,2,0:T(8,128)(2,1)} all-to-all(bf16[4,64,1,12,512]{4,1,3,2,0:T(8,128)(2,1)S(1)} %bitcast.163), channel_id=1, replica_groups=mesh['sp'=64,'tp'=4] {'tp'}, dimensions={0} | all-to-all | bytes 6291456 | tf_op jit(solution)/shard_map/all_to_all | solution.py:23
  160.3 3.5 %reduce_sum.48 = bf16[64,12,512]{2,0,1:T(8,128)(2,1)} reduce(bf16[4,64,1,12,512]{4,1,3,2,0:T(8,128)(2,1)} %all_to_all.26, bf16[]{:T(256)} %constant.12.clone.1), dimensions={0,2}, to_apply=%region_4.5 | reduce | flops 1179648 | bytes 3932162 | tf_op jit(solution)/shard_map/reduce_sum | solution.py:24
  163.8 2.5 copy.54
  166.3 9.5 %all-to-all-start.3 = ((bf16[64,1,12,512]{3,2,1,0:T(8,128)(2,1)}), bf16[64,1,12,512]{3,2,1,0:T(8,128)(2,1)}, u32[]{:S(2)}, u32[]{:S(2)}) async-start(bf16[64,1,12,512]{3,2,1,0:T(8,128)(2,1)} %copy.54), calls=%async_computation.3 | async-start | bytes 2097152 | tf_op jit(solution)/shard_map/all_to_all | solution.py:98
  175.9 3.5 %collective-permute-start = (bf16[2,2,256]{2,1,0:T(2,128)(2,1)S(1)}, bf16[2,2,256]{2,1,0:T(2,128)(2,1)S(1)}, u32[]{:S(2)}, u32[]{:S(2)}) collective-permute-start(bf16[2,2,256]{2,1,0:T(2,128)(2,1)S(1)} %pad_maximum_fusion.2), channel_id=1, source_target_pairs={{0,4},{4,8},{8,12},{12,16},{16,20},{20,24},{24,28},{28,32},{32,36}... | collective-permute-start | bytes 6152 | tf_op jit(solution)/shard_map/ppermute | solution.py:30
  181.7 22.2 %all-to-all-done.3 = bf16[64,1,12,512]{3,2,1,0:T(8,128)(2,1)} async-done(((bf16[64,1,12,512]{3,2,1,0:T(8,128)(2,1)}), bf16[64,1,12,512]{3,2,1,0:T(8,128)(2,1)}, u32[]{:S(2)}, u32[]{:S(2)}) %all-to-all-start.3) | async-done | bytes 786464 | tf_op jit(solution)/shard_map/all_to_all | solution.py:98
  203.9 2.1 reshape.161
  206.0 3.3 %gather_fusion = bf16[384,512]{1,0:T(8,128)(2,1)S(1)} fusion(bf16[768,512]{1,0:T(8,128)(2,1)} %reshape.161, s32[1024]{0:T(1024)S(1)} %pad_clamp_fusion), kind=kCustom, calls=%fused_computation | custom fusion | bytes 787968 | tf_op jit(solution)/shard_map/jit(_take)/gather | solution.py:103
  210.2 2.2 convert_reduce_fusion.1
  213.4 11.0 %all_gather.3 = bf16[192,2048]{1,0:T(8,128)(2,1)S(1)} all-gather(bf16[192,512]{1,0:T(8,128)(2,1)S(1)} %add_convert_fusion.1), channel_id=1, replica_groups=mesh['sp'=64,'tp'=4] {'tp'}, dimensions={1}, use_global_device_ids=true | all-gather | bytes 983040 | tf_op jit(solution)/shard_map/all_gather | solution.py:110
  224.4 2.5 multiply_convert_fusion.6
  228.3 9.5 %all-to-all-start.4 = ((bf16[64,32,256]{2,1,0:T(8,128)(2,1)}), bf16[64,32,256]{2,1,0:T(8,128)(2,1)}, u32[]{:S(2)}, u32[]{:S(2)}) async-start(bf16[64,32,256]{2,1,0:T(8,128)(2,1)} %bitcast.167), calls=%async_computation.4 | async-start | bytes 2097152 | tf_op jit(solution)/shard_map/all_to_all | solution.py:23
  237.8 3.1 %fusion.33 = bf16[1,2048,256]{1,2,0:T(8,128)(2,1)} fusion(bf16[64,1,12,2048]{3,0,2,1:T(8,128)(2,1)S(1)} %copy-done, bf16[64,1,12,256]{3,0,2,1:T(8,128)(2,1)} %copy-done.12), kind=kOutput, calls=%fused_computation.25 | convolution fusion | flops 805830656 | bytes 4587520 | tf_op jit(solution)/shard_map/secd,secf->edf/dot_general | solution.py:85
  240.9 4.0 %fusion.30 = bf16[1,256,2048]{2,1,0:T(8,128)(2,1)} fusion(bf16[64,1,12,2048]{3,0,1,2:T(8,128)(2,1)} %all-to-all-done.1, f32[64,1,12,256]{3,0,2,1:T(8,128)S(1)} %copy-done.18, f32[64,1,12,256]{3,0,2,1:T(8,128)S(1)} %copy-done.17), kind=kOutput, calls=%fused_computation.24 | convolution fusion | flops 807010304 | bytes 5767168 | tf_op jit(solution)/shard_map/secf,secd->efd/dot_general | solution.py:82
  245.5 2.5 collective-permute-start.1
  248.1 2.0 fusion.36
  250.0 2.3 copy.55
  252.3 2.3 copy.56
  256.0 10.0 %all-to-all-done.4 = bf16[64,32,256]{2,1,0:T(8,128)(2,1)} async-done(((bf16[64,32,256]{2,1,0:T(8,128)(2,1)}), bf16[64,32,256]{2,1,0:T(8,128)(2,1)}, u32[]{:S(2)}, u32[]{:S(2)}) %all-to-all-start.4) | async-done | bytes 1048608 | tf_op jit(solution)/shard_map/all_to_all | solution.py:23
  266.0 2.0 convert_reduce_fusion
  (74 shorter events, 15.0 us)
Async XLA Ops:
  0.6 77.7 %copy-start = (bf16[64,1,12,2048]{3,0,2,1:T(8,128)(2,1)S(1)}, bf16[64,1,12,2048]{3,0,2,1:T(8,128)(2,1)}, u32[]{:S(2)}) copy-start(bf16[64,1,12,2048]{3,0,2,1:T(8,128)(2,1)} %param.15) | copy-start | bytes 9437188
  8.6 5.3 %copy-start.16 = (f32[192,2]{0,1:T(2,128)S(1)}, f32[192,2]{0,1:T(2,128)}, u32[]{:S(2)}) copy-start(f32[192,2]{0,1:T(2,128)} %param.14) | copy-start | bytes 4612
  73.5 41.2 %all-to-all-start.1 = ((bf16[64,1,12,2048]{3,0,1,2:T(8,128)(2,1)}), bf16[64,1,12,2048]{3,0,1,2:T(8,128)(2,1)}, u32[]{:S(2)}, u32[]{:S(2)}) async-start(bf16[64,1,12,2048]{3,0,1,2:T(8,128)(2,1)} %bitcast.164), calls=%async_computation.1 | async-start | bytes 6291456 | tf_op jit(solution)/shard_map/all_to_all | solution.py:10
  78.4 3.2 %copy-start.2 = (bf16[1,2048,256]{2,1,0:T(8,128)(2,1)S(1)}, bf16[1,2048,256]{2,1,0:T(8,128)(2,1)}, u32[]{:S(2)}) copy-start(bf16[1,2048,256]{2,1,0:T(8,128)(2,1)} %param.17) | copy-start | bytes 3145732
  114.7 3.9 %copy-start.1 = (bf16[1,2048,256]{2,1,0:T(8,128)(2,1)S(1)}, bf16[1,2048,256]{2,1,0:T(8,128)(2,1)}, u32[]{:S(2)}) copy-start(bf16[1,2048,256]{2,1,0:T(8,128)(2,1)} %param.16) | copy-start | bytes 3145732
  118.6 1.1 copy-start.12
  118.6 1.1 copy-start.10
  118.7 1.5 copy-start.3
  160.3 15.6 %copy-start.5 = (bf16[192,256]{1,0:T(8,128)(2,1)S(1)}, bf16[192,256]{1,0:T(8,128)(2,1)}, u32[]{:S(2)}) copy-start(bf16[192,256]{1,0:T(8,128)(2,1)} %param.19) | copy-start | bytes 294916
  160.3 15.6 %copy-start.7 = (bf16[192,256]{1,0:T(8,128)(2,1)S(1)}, bf16[192,256]{1,0:T(8,128)(2,1)}, u32[]{:S(2)}) copy-start(bf16[192,256]{1,0:T(8,128)(2,1)} %param.21) | copy-start | bytes 294916
  160.3 19.4 %copy-start.13 = (s32[192,2]{0,1:T(2,128)S(1)}, s32[192,2]{0,1:T(2,128)}, u32[]{:S(2)}) copy-start(s32[192,2]{0,1:T(2,128)} %param.13) | copy-start | bytes 4612
  160.3 19.4 %copy-start.15 = (f32[3,256]{1,0:T(4,128)S(1)}, f32[3,256]{1,0:T(4,128)}, u32[]{:S(2)}) copy-start(f32[3,256]{1,0:T(4,128)} %param.22) | copy-start | bytes 9220
  166.3 37.6 %all-to-all-start.3 = ((bf16[64,1,12,512]{3,2,1,0:T(8,128)(2,1)}), bf16[64,1,12,512]{3,2,1,0:T(8,128)(2,1)}, u32[]{:S(2)}, u32[]{:S(2)}) async-start(bf16[64,1,12,512]{3,2,1,0:T(8,128)(2,1)} %copy.54), calls=%async_computation.3 | async-start | bytes 2097152 | tf_op jit(solution)/shard_map/all_to_all | solution.py:98
  175.9 5.3 %collective-permute-start = (bf16[2,2,256]{2,1,0:T(2,128)(2,1)S(1)}, bf16[2,2,256]{2,1,0:T(2,128)(2,1)S(1)}, u32[]{:S(2)}, u32[]{:S(2)}) collective-permute-start(bf16[2,2,256]{2,1,0:T(2,128)(2,1)S(1)} %pad_maximum_fusion.2), channel_id=1, source_target_pairs={{0,4},{4,8},{8,12},{12,16},{16,20},{20,24},{24,28},{28,32},{32,36}... | collective-permute-start | bytes 6152 | tf_op jit(solution)/shard_map/ppermute | solution.py:30
  209.3 15.1 %copy-start.14 = (f32[2,256]{1,0:T(2,128)S(1)}, f32[2,256]{1,0:T(2,128)}, u32[]{:S(2)}) copy-start(f32[2,256]{1,0:T(2,128)} %multiply_bitcast_fusion) | copy-start | bytes 6148
  210.2 16.6 %copy-start.9 = (bf16[192,256]{1,0:T(8,128)(2,1)S(1)}, bf16[192,256]{1,0:T(8,128)(2,1)}, u32[]{:S(2)}) copy-start(bf16[192,256]{1,0:T(8,128)(2,1)} %param.20) | copy-start | bytes 294916
  213.4 14.9 %copy-start.4 = (bf16[192,512]{1,0:T(8,128)(2,1)}, bf16[192,512]{1,0:T(8,128)(2,1)S(1)}, u32[]{:S(2)}) copy-start(bf16[192,512]{1,0:T(8,128)(2,1)S(1)} %add_convert_fusion.1) | copy-start | bytes 589828
  228.3 37.7 %all-to-all-start.4 = ((bf16[64,32,256]{2,1,0:T(8,128)(2,1)}), bf16[64,32,256]{2,1,0:T(8,128)(2,1)}, u32[]{:S(2)}, u32[]{:S(2)}) async-start(bf16[64,32,256]{2,1,0:T(8,128)(2,1)} %bitcast.167), calls=%async_computation.4 | async-start | bytes 2097152 | tf_op jit(solution)/shard_map/all_to_all | solution.py:23
  237.8 3.1 %copy-start.17 = (f32[64,1,12,256]{3,0,2,1:T(8,128)S(1)}, f32[64,1,12,256]{3,0,2,1:T(8,128)}, u32[]{:S(2)}) copy-start(f32[64,1,12,256]{3,0,2,1:T(8,128)} %fusion.48) | copy-start | bytes 2359300
  237.8 3.1 %copy-start.18 = (f32[64,1,12,256]{3,0,2,1:T(8,128)S(1)}, f32[64,1,12,256]{3,0,2,1:T(8,128)}, u32[]{:S(2)}) copy-start(f32[64,1,12,256]{3,0,2,1:T(8,128)} %fusion.45) | copy-start | bytes 2359300
  240.9 7.1 %copy-start.11 = (bf16[64,1,12,256]{3,0,2,1:T(8,128)(2,1)S(1)}, bf16[64,1,12,256]{3,0,2,1:T(8,128)(2,1)}, u32[]{:S(2)}) copy-start(bf16[64,1,12,256]{3,0,2,1:T(8,128)(2,1)} %copy-done.10) | copy-start | bytes 1179652
  245.5 9.1 %collective-permute-start.1 = (f32[2,256]{1,0:T(2,128)}, f32[2,256]{1,0:T(2,128)S(1)}, u32[]{:S(2)}, u32[]{:S(2)}) collective-permute-start(f32[2,256]{1,0:T(2,128)} %slice.66), channel_id=1, source_target_pairs={{4,0},{8,4},{12,8},{16,12},{20,16},{24,20},{28,24},{32,28},{36,32}... | collective-permute-start | bytes 6152 | tf_op jit(solution)/shard_map/ppermute | solution.py:30
  250.0 4.6 %copy-start.6 = (bf16[192,256]{1,0:T(8,128)(2,1)S(1)}, bf16[192,256]{1,0:T(8,128)(2,1)}, u32[]{:S(2)}) copy-start(bf16[192,256]{1,0:T(8,128)(2,1)} %param.19) | copy-start | bytes 294916
  250.0 5.3 %copy-start.8 = (bf16[192,256]{1,0:T(8,128)(2,1)S(1)}, bf16[192,256]{1,0:T(8,128)(2,1)}, u32[]{:S(2)}) copy-start(bf16[192,256]{1,0:T(8,128)(2,1)} %param.21) | copy-start | bytes 294916
